TPU v7x, 512 devices: a whole 4x4x16 slice. The times are simulated.
512 devices in a mesh: fs: 64 (over z, y), tp: 8 (over x, core).
Axes of the slice: x: 4, y: 4, z: 16, core: 2. Of those that a mesh axis runs over, the one named last changes fastest.
Arguments:
- tokens: bfloat16 [20480, 2048], P('fs'), may hold values from -6 to 6
- w_gate: bfloat16 [2048, 5632], P('fs', 'tp'), may hold values from -0.125 to 0.125
- w_up: bfloat16 [2048, 5632], P('fs', 'tp'), may hold values from -0.125 to 0.125
- w_down: bfloat16 [5632, 2048], P('tp', 'fs'), may hold values from -0.078125 to 0.078125
- w_mix_in: bfloat16 [2048, 1024], P('fs', 'tp'), may hold values from -0.125 to 0.125
- w_mix_out: bfloat16 [1024, 2048], P('tp', 'fs'), may hold values from -0.1875 to 0.1875
- pool_w: bfloat16 [8, 128, 128], P('tp'), may hold values from -0.5 to 0.5
- pool_scale: bfloat16 [1024], P('tp'), may hold values from 0.099609375 to 1.8984375
- norm_gains: float32 [6, 2048], replicated, may hold values from 0.1 to 1.9
Outputs:
- layer_out: bfloat16 [20480, 2048], P(('fs', 'tp'))
All inputs are finite; a program needn't handle non-finite values.
Results may differ from a plain program's by a relative error of at most 0.018.
Values may be sent and summed in bfloat16 or wider, within the bound.
No kernel may reach another device: no remote copies, remote signals or barrier semaphores. Data moves between devices by JAX's collectives and lax.ppermute only.
A program may use at most 64 MiB of HBM per device.

v0:
```python
import jax
import jax.numpy as jnp
from jax import lax
from jax.sharding import PartitionSpec as P

LEN = 64


def in_blocks(array, dim, peers):
    shape = array.shape
    tiles = array.reshape(*shape[:dim], peers, shape[dim] // peers, *shape[dim + 1 :])
    return jnp.moveaxis(tiles, dim, 0)


def sum_at_owner(array, axis, dim):
    peers = lax.axis_size(axis)
    tiles = lax.all_to_all(in_blocks(array, dim, peers), axis, 0, 0, tiled=True)
    return jnp.sum(tiles.astype(jnp.float32), axis=0)


def sent_to_all(array, axis):
    peers = lax.axis_size(axis)
    return lax.all_to_all(
        jnp.broadcast_to(array[None], (peers, *array.shape)), axis, 0, 0, tiled=True
    )


def in_order(tiles, dim):
    shape = list(tiles.shape[1:])
    shape[dim] *= tiles.shape[0]
    return jnp.moveaxis(tiles, 0, dim).reshape(shape)


def gathered_copies(array, axis, dim):
    tiles = sent_to_all(array, axis)
    return in_order(tiles, dim)


def rows_first(arrays, axis, dims):
    turned = [jnp.moveaxis(a, dim, 0) for a, dim in zip(arrays, dims)]
    both = jnp.concatenate([t.reshape(len(t), -1) for t in turned], axis=1)
    out, at, done = (lax.all_gather(both, axis, axis=0, tiled=True), 0, [])
    for t, dim in zip(turned, dims):
        share = out[:, at : at + t[0].size].reshape(-1, *t.shape[1:])
        done.append(jnp.moveaxis(share, 0, dim))
        at += t[0].size
    return tuple(done)


def sent_together(arrays, axis, dim, along):
    widths = [a.shape[along] for a in arrays]
    both = jnp.concatenate(arrays, axis=along)
    out = lax.all_gather(both, axis, axis=dim, tiled=True)
    return tuple(jnp.split(out, [sum(widths[:k]) for k in range(1, len(widths))], axis=along))


def rms_scale(values, gain):
    return values * lax.rsqrt(jnp.mean(values * values, axis=-1, keepdims=True) + 1e-06) * gain


def reduce_rows(left_rows, right_matrix):
    return sum_at_owner(
        jnp.dot(left_rows, right_matrix, preferred_element_type=jnp.float32).astype(jnp.bfloat16),
        "tp",
        0,
    )


def gather_rows(normed, project):
    return project(gathered_copies(normed, "tp", 0), jnp.int32(0))


def body(tokens, w_gate, w_up, w_down, w_mix_in, w_mix_out, pool_w, pool_scale, norm_gains):
    tp_size = lax.axis_size("tp")
    rows_all = tokens.shape[0]
    own_rows = rows_all // tp_size
    stream = tokens.astype(jnp.float32)
    normed = rms_scale(stream, norm_gains[0]).astype(jnp.bfloat16)
    down_full, mix_in_full, mix_out_full = rows_first(
        (w_down, w_mix_in, w_mix_out), "fs", (1, 0, 1)
    )
    gate_full, up_full = sent_together((w_gate, w_up), "fs", 0, 1)
    gate_first = jnp.dot(normed, gate_full, preferred_element_type=jnp.float32)
    up_first = jnp.dot(normed, up_full, preferred_element_type=jnp.float32)
    hidden = (jax.nn.silu(gate_first) * up_first).astype(jnp.bfloat16)
    stream_own = lax.dynamic_slice_in_dim(stream, lax.axis_index("tp") * own_rows, own_rows, 0)
    stream_own = stream_own + 0.5 * rms_scale(reduce_rows(hidden, down_full), norm_gains[1])
    normed = rms_scale(stream_own, norm_gains[2]).astype(jnp.bfloat16)

    def project_pool(part_rows, offset):
        return jnp.dot(part_rows, mix_in_full, preferred_element_type=jnp.float32).astype(
            jnp.bfloat16
        )

    pooled_in = gather_rows(normed, project_pool)
    groups_here = pool_w.shape[0]
    group_dim = pool_w.shape[1]
    values = pooled_in.astype(jnp.float32).reshape(rows_all // LEN, LEN, groups_here, group_dim)
    totals = jnp.cumsum(values, axis=1)
    position = jnp.arange(1, LEN + 1).astype(jnp.float32)[None, :, None, None]
    window_ids = (lax.axis_index("tp") * groups_here + jnp.arange(groups_here)) % 4
    average = jnp.zeros_like(values)
    for window_slot in range(4):
        window = 2 ** (1 + window_slot)
        lagged = jnp.pad(totals, ((0, 0), (window, 0), (0, 0), (0, 0)))[:, :LEN]
        candidate = (totals - lagged) / jnp.minimum(position, float(window))
        average = jnp.where((window_ids == window_slot)[None, None, :, None], candidate, average)
    deviation = (average - values).astype(jnp.bfloat16)
    regrouped = jnp.einsum("btgi,gio->btgo", deviation, pool_w, preferred_element_type=jnp.float32)
    regrouped = (
        regrouped.reshape(rows_all, groups_here * group_dim) * pool_scale.astype(jnp.float32)
    ).astype(jnp.bfloat16)
    stream_own = stream_own + rms_scale(reduce_rows(regrouped, mix_out_full), norm_gains[3])
    normed = rms_scale(stream_own, norm_gains[4]).astype(jnp.bfloat16)

    def project_ffn(part_rows, offset):
        gate_part = jnp.dot(part_rows, gate_full, preferred_element_type=jnp.float32)
        up_part = jnp.dot(part_rows, up_full, preferred_element_type=jnp.float32)
        return (jax.nn.silu(gate_part) * up_part).astype(jnp.bfloat16)

    hidden = gather_rows(normed, project_ffn)
    stream_own = stream_own + 0.5 * rms_scale(reduce_rows(hidden, down_full), norm_gains[5])
    return stream_own.astype(jnp.bfloat16)


def solution(mesh):
    in_specs = (
        P("fs", None),
        P("fs", "tp"),
        P("fs", "tp"),
        P("tp", "fs"),
        P("fs", "tp"),
        P("tp", "fs"),
        P("tp", None, None),
        P("tp"),
        P(),
    )
    out_specs = P(("fs", "tp"), None)
    return jax.shard_map(body, mesh=mesh, in_specs=in_specs, out_specs=out_specs, check_vma=False)
```

profile of v0, /device:TPU:1, one launch (start us, length us, event | category | flops | bytes accessed | tf_op | source)
XLA Modules:
  0.0 450.3 jit_solution(10392852320898855654)
XLA Ops:
  6.5 0.0 copy-start
  6.5 0.0 all-gather.3.cloned.1.call-start
  6.5 1.6 pad_maximum_fusion
  8.1 0.0 all-gather.3.cloned.1.call-update
  8.1 0.0 all-gather.5.cloned.1.call-start
  8.2 1.5 pad_maximum_fusion.1
  9.7 0.0 all-gather.5.cloned.1.call-update
  9.7 1.7 multiply_reduce_fusion
  11.4 1.1 fusion.49
  12.6 144.5 %all-gather.3.cloned.1.call-done = bf16[2048,1408]{1,0:T(8,128)(2,1)} async-done(((bf16[32,1408]{1,0:T(8,128)(2,1)}), bf16[2048,1408]{1,0:T(8,128)(2,1)}) %all-gather.3.cloned.1.call-update) | async-done | bytes 5767184 | tf_op jit(solution)/shard_map/all_gather | solution.py:53
  157.1 0.0 copy-start.1
  157.1 3.6 fusion.10
  160.7 139.5 %all-gather.5.cloned.1.call-done = bf16[2048,960]{1,0:T(8,128)(2,1)} async-done(((bf16[32,960]{1,0:T(8,128)(2,1)}), bf16[2048,960]{1,0:T(8,128)(2,1)}) %all-gather.5.cloned.1.call-update) | async-done | bytes 3932176 | tf_op jit(solution)/shard_map/all_gather | solution.py:42
  300.2 0.0 copy-done.1
  300.2 7.0 %fusion.12 = bf16[320,2048]{1,0:T(8,128)(2,1)} fusion(bf16[2048,960]{1,0:T(8,128)(2,1)} %all-gather.5.cloned.1.call-done, bf16[2048,1408]{1,0:T(8,128)(2,1)} %all-gather.3.cloned.1.call-done, f32[320,704]{1,0:T(8,128)S(1)} %fusion.10, f32[2048]{0:T(1024)S(1)} %bitcast.61, f32[320]{0:T(512)S(1)} %add_rsqrt_fusion, bf16[320,2048]{1,0:T(8,128)(2,1)S(1)} %copy-done.1), kind=kOutput, calls=%fused_computation.13 | convolution fusion | flops 1850122240 | bytes 9823488 | tf_op jit(solution)/shard_map/dot_general | solution.py:63
  307.2 13.9 %all-to-all-start = ((bf16[8,40,2048]{2,1,0:T(8,128)(2,1)}), bf16[8,40,2048]{2,1,0:T(8,128)(2,1)S(1)}, u32[]{:S(2)}, u32[]{:S(2)}) async-start(bf16[8,40,2048]{2,1,0:T(8,128)(2,1)} %bitcast.48), calls=%async_computation | async-start | bytes 2621440 | tf_op jit(solution)/shard_map/all_to_all | solution.py:17
  321.1 1.8 convert_element_type.82
  322.9 16.0 %all-to-all-done = bf16[8,40,2048]{2,1,0:T(8,128)(2,1)S(1)} async-done(((bf16[8,40,2048]{2,1,0:T(8,128)(2,1)}), bf16[8,40,2048]{2,1,0:T(8,128)(2,1)S(1)}, u32[]{:S(2)}, u32[]{:S(2)}) %all-to-all-start) | async-done | bytes 1310752 | tf_op jit(solution)/shard_map/all_to_all | solution.py:17
  338.9 0.2 convert_reduce_fusion.2
  339.1 0.1 multiply_reduce_fusion.5
  339.2 0.0 copy-start.2
  339.2 1.2 multiply_reduce_fusion.4
  340.5 0.1 multiply_convert_fusion.5
  340.6 1.2 broadcast_in_dim.60
  341.8 4.4 all-to-all-start.1
  346.2 0.0 copy-done.2
  346.3 17.8 %all-to-all-done.1 = bf16[8,40,2048]{2,1,0:T(8,128)(2,1)S(1)} async-done(((bf16[8,40,2048]{2,1,0:T(8,128)(2,1)}), bf16[8,40,2048]{2,1,0:T(8,128)(2,1)S(1)}, u32[]{:S(2)}, u32[]{:S(2)}) %all-to-all-start.1) | async-done | bytes 1310752 | tf_op jit(solution)/shard_map/all_to_all | solution.py:23
  364.0 1.8 convolution_convert_fusion.1
  365.9 0.1 fusion.50
  366.0 1.7 subtract_convert_fusion
  367.7 0.0 copy-done
  367.7 0.2 fusion.43
  367.9 0.0 slice-start
  367.9 2.0 convolution_convert_fusion
  369.9 21.1 %all_to_all.25 = bf16[8,40,2048]{2,1,0:T(8,128)(2,1)S(1)} all-to-all(bf16[8,40,2048]{2,1,0:T(8,128)(2,1)S(1)} %bitcast.44), channel_id=1, replica_groups=mesh['fs'=64,'tp'=8] {'tp'}, dimensions={0} | all-to-all | bytes 2621440 | tf_op jit(solution)/shard_map/all_to_all | solution.py:17
  391.0 0.0 slice-start.1
  391.0 0.2 convert_reduce_fusion.1
  391.2 0.1 multiply_reduce_fusion.3
  391.3 0.2 multiply_reduce_fusion.2
  391.6 0.1 multiply_convert_fusion.4
  391.7 0.1 broadcast_in_dim.68
  391.8 21.2 %all_to_all.26 = bf16[8,40,2048]{2,1,0:T(8,128)(2,1)S(1)} all-to-all(bf16[8,40,2048]{2,1,0:T(8,128)(2,1)S(1)} %broadcast_in_dim.68), channel_id=1, replica_groups=mesh['fs'=64,'tp'=8] {'tp'}, dimensions={0} | all-to-all | bytes 2621440 | tf_op jit(solution)/shard_map/all_to_all | solution.py:23
  413.1 0.0 slice-done
  413.1 0.0 slice-done.1
  413.1 2.2 fusion.8
  415.3 5.9 %fusion.15 = bf16[320,2048]{1,0:T(8,128)(2,1)S(1)} fusion(bf16[2048,960]{1,0:T(8,128)(2,1)} %all-gather.5.cloned.1.call-done, bf16[320,2048]{1,0:T(8,128)(2,1)S(1)} %bitcast.50, bf16[2048,1408]{1,0:T(8,128)(2,1)} %all-gather.3.cloned.1.call-done, f32[320,704]{1,0:T(8,128)} %fusion.8), kind=kOutput, calls=%fused_computation.14 | convolution fusion | flops 1847500800 | bytes 9895936 | tf_op jit(solution)/shard_map/dot_general | solution.py:63
  421.2 21.2 %all_to_all.27 = bf16[8,40,2048]{2,1,0:T(8,128)(2,1)S(1)} all-to-all(bf16[8,40,2048]{2,1,0:T(8,128)(2,1)S(1)} %bitcast.51), channel_id=1, replica_groups=mesh['fs'=64,'tp'=8] {'tp'}, dimensions={0} | all-to-all | bytes 2621440 | tf_op jit(solution)/shard_map/all_to_all | solution.py:17
  442.4 0.2 convert_reduce_fusion
  442.6 0.1 multiply_reduce_fusion.1
  442.7 0.8 add_convert_fusion
  (12 shorter events, 0.1 us)
Async XLA Ops:
  6.5 361.1 %copy-start = (bf16[1,128,128]{2,1,0:T(8,128)(2,1)S(1)}, bf16[1,128,128]{2,1,0:T(8,128)(2,1)}, u32[]{:S(2)}) copy-start(bf16[1,128,128]{2,1,0:T(8,128)(2,1)} %param.15) | copy-start | bytes 98308
  6.5 150.6 %all-gather.3.cloned.1.call-start = ((), (), s32[]{:S(2)}) async-start(), calls=%async_computation.5 | async-start | bytes 5857280 | tf_op jit(solution)/shard_map/all_gather | solution.py:53
  8.1 292.1 %all-gather.5.cloned.1.call-start = ((), (), s32[]{:S(2)}) async-start(), calls=%async_computation.6 | async-start | bytes 4259840 | tf_op jit(solution)/shard_map/all_gather | solution.py:42
  157.1 143.1 %copy-start.1 = (bf16[320,2048]{1,0:T(8,128)(2,1)S(1)}, bf16[320,2048]{1,0:T(8,128)(2,1)}, u32[]{:S(2)}) copy-start(bf16[320,2048]{1,0:T(8,128)(2,1)} %param.9) | copy-start | bytes 3932164
  307.2 31.7 %all-to-all-start = ((bf16[8,40,2048]{2,1,0:T(8,128)(2,1)}), bf16[8,40,2048]{2,1,0:T(8,128)(2,1)S(1)}, u32[]{:S(2)}, u32[]{:S(2)}) async-start(bf16[8,40,2048]{2,1,0:T(8,128)(2,1)} %bitcast.48), calls=%async_computation | async-start | bytes 2621440 | tf_op jit(solution)/shard_map/all_to_all | solution.py:17
  339.2 7.0 %copy-start.2 = (bf16[128]{0:T(256)(128)(2,1)S(1)}, bf16[128]{0:T(256)(128)(2,1)}, u32[]{:S(2)}) copy-start(bf16[128]{0:T(256)(128)(2,1)} %param.16) | copy-start | bytes 772
  341.8 22.2 %all-to-all-start.1 = ((bf16[8,40,2048]{2,1,0:T(8,128)(2,1)}), bf16[8,40,2048]{2,1,0:T(8,128)(2,1)S(1)}, u32[]{:S(2)}, u32[]{:S(2)}) async-start(bf16[8,40,2048]{2,1,0:T(8,128)(2,1)} %broadcast_in_dim.60), calls=%async_computation.1 | async-start | bytes 2621440 | tf_op jit(solution)/shard_map/all_to_all | solution.py:23
  367.9 45.2 %slice-start = ((s8[5767168]{0:T(1024)(128)(4,1)}), s8[4194304]{0:T(1024)(128)(4,1)S(1)}, s32[]{:S(2)}) async-start(s8[5767168]{0:T(1024)(128)(4,1)} %bitcast.62), calls=%async_computation.7 | async-start | bytes 8388608
  391.0 22.1 %slice-start.1 = ((s8[5767168]{0:T(1024)(128)(4,1)}), s8[1572864]{0:T(1024)(128)(4,1)S(1)}, s32[]{:S(2)}) async-start(s8[5767168]{0:T(1024)(128)(4,1)} %bitcast.62), calls=%async_computation.8 | async-start | bytes 3145728
Sparse Core Ops, SparseCore 0:
  10.3 146.7 all-gather.2
  160.0 140.1 all-gather.4
where the time goes:
time: 451 us; the launch traced here: 450 us
  waiting for transfers between devices  318 us (71%)
  blocking collectives  63.5 us (14%)
  matrix products  22.6 us (5%)
  starting transfers between devices  18.4 us (4%)
  between operations  13.6 us (3%)
  other arithmetic  11.9 us (3%)
    all_gather x1, waiting for transfers between devices, sent_together(): out = lax.all_gather(both, axis, axis=dim, tiled=True)  145 us
    all_gather x1, waiting for transfers between devices, rows_first(): out, at, done = (lax.all_gather(both, axis, axis=0, tiled=True), 0, [])  140 us
    all_to_all x2, blocking collectives, sum_at_owner(): tiles = lax.all_to_all(in_blocks(array, dim, peers), axis, 0, 0, tiled=True)  42.3 us
    all_to_all x1, blocking collectives, sent_to_all(): lax.all_to_all(jnp.broadcast_to(array[None], (peers, *array.shape)), axis...  21.2 us
    all_to_all x1, waiting for transfers between devices, sent_to_all(): lax.all_to_all(jnp.broadcast_to(array[None], (peers, *array.shape)), axis...  17.8 us
    all_to_all x1, waiting for transfers between devices, sum_at_owner(): tiles = lax.all_to_all(in_blocks(array, dim, peers), axis, 0, 0, tiled=True)  16 us
    dot_general x3, matrix products, reduce_rows(): jnp.dot(left_rows, right_matrix, preferred_element_type=jnp.float32)  14.8 us
    all_to_all x1, starting transfers between devices, sum_at_owner(): tiles = lax.all_to_all(in_blocks(array, dim, peers), axis, 0, 0, tiled=True)  13.9 us
  transfers between devices with their start and end apart: 4, of which 4 were waited for; matrix products, arithmetic and copies ran while one was open for 2% of the time, Pallas kernels for 0%

commit v1 on v0

--- a/solution.py
+++ b/solution.py
@@ -4,6 +4,13 @@
 from jax.sharding import PartitionSpec as P
 
 LEN = 64
+
+
+def hold_weights(here_x, net_axis):
+    return jnp.concatenate(
+        lax.all_to_all(jnp.stack([here_x for _ in range(lax.axis_size(net_axis))]), net_axis, 0, 0),
+        axis=0,
+    )
 
 
 def in_blocks(array, dim, peers):
@@ -39,7 +46,7 @@
 def rows_first(arrays, axis, dims):
     turned = [jnp.moveaxis(a, dim, 0) for a, dim in zip(arrays, dims)]
     both = jnp.concatenate([t.reshape(len(t), -1) for t in turned], axis=1)
-    out, at, done = (lax.all_gather(both, axis, axis=0, tiled=True), 0, [])
+    out, at, done = (hold_weights(both, axis), 0, [])
     for t, dim in zip(turned, dims):
         share = out[:, at : at + t[0].size].reshape(-1, *t.shape[1:])
         done.append(jnp.moveaxis(share, 0, dim))

time: 451 us -> 405 us (0.90)
  waiting for transfers between devices: 318 us -> 259 us
  starting transfers between devices: 18.4 us -> 32.3 us
    all_gather x1 -> x0, waiting for transfers between devices: 140 us -> none  [rows_first(): out, at, done = (lax.all_gather(both, axis, axis=0, tiled=True), 0, [])]
    all_gather x1, waiting for transfers between devices: 145 us -> 226 us  [sent_together(): out = lax.all_gather(both, axis, axis=dim, tiled=True)]
    all_to_all x0 -> x1, starting transfers between devices: none -> 19.7 us  [hold_weights(): lax.all_to_all(jnp.stack([here_x for _ in range(lax.axis_size(net_axis))]...]
    all_to_all x1, starting transfers between devices: 13.9 us -> 8.19 us  [sum_at_owner(): tiles = lax.all_to_all(in_blocks(array, dim, peers), axis, 0, 0, tiled=True)]
  transfers between devices with their start and end apart: 4 -> 4, of which waited for: 4 -> 3; matrix products, arithmetic and copies ran while one was open for 2% -> 1% of each run, Pallas kernels for 0% -> 0%
where the time goes in v1:
time: 405 us; the launch traced here: 404 us
  waiting for transfers between devices  259 us (64%)
  blocking collectives  63.6 us (16%)
  starting transfers between devices  32.3 us (8%)
  matrix products  22.1 us (5%)
  between operations  13.6 us (3%)
  other arithmetic  9.09 us (2%)
    all_gather x1, waiting for transfers between devices, sent_together(): out = lax.all_gather(both, axis, axis=dim, tiled=True)  226 us
    all_to_all x2, blocking collectives, sum_at_owner(): tiles = lax.all_to_all(in_blocks(array, dim, peers), axis, 0, 0, tiled=True)  42.4 us
    all_to_all x1, blocking collectives, sent_to_all(): lax.all_to_all(jnp.broadcast_to(array[None], (peers, *array.shape)), axis...  21.2 us
    all_to_all x1, starting transfers between devices, hold_weights(): lax.all_to_all(jnp.stack([here_x for _ in range(lax.axis_size(net_axis))]...  19.7 us
    all_to_all x1, waiting for transfers between devices, sent_to_all(): lax.all_to_all(jnp.broadcast_to(array[None], (peers, *array.shape)), axis...  17.8 us
    all_to_all x1, waiting for transfers between devices, sum_at_owner(): tiles = lax.all_to_all(in_blocks(array, dim, peers), axis, 0, 0, tiled=True)  16 us
    dot_general x3, matrix products, reduce_rows(): jnp.dot(left_rows, right_matrix, preferred_element_type=jnp.float32)  14.8 us
    all_to_all x1, starting transfers between devices, sum_at_owner(): tiles = lax.all_to_all(in_blocks(array, dim, peers), axis, 0, 0, tiled=True)  8.19 us
  transfers between devices with their start and end apart: 4, of which 3 were waited for; matrix products, arithmetic and copies ran while one was open for 1% of the time, Pallas kernels for 0%

profile of v1, /device:TPU:1, one launch (start us, length us, event | category | flops | bytes accessed | tf_op | source)
XLA Modules:
  0.0 404.0 jit_solution(2548190443062991759)
XLA Ops:
  6.5 0.0 copy-start
  6.5 0.9 pad_maximum_fusion.1
  7.5 2.6 stack.2
  10.1 0.0 copy-start.2
  10.1 0.0 copy-start.3
  10.1 0.0 copy-start.1
  10.1 0.0 copy-start.4
  10.1 19.7 %all-to-all-start = ((bf16[64,32,960]{2,1,0:T(8,128)(2,1)}), bf16[64,32,960]{2,1,0:T(8,128)(2,1)}, u32[]{:S(2)}, u32[]{:S(2)}) async-start(bf16[64,32,960]{2,1,0:T(8,128)(2,1)} %stack.2), calls=%async_computation | async-start | bytes 8388608 | tf_op jit(solution)/shard_map/all_to_all | solution.py:11
  29.8 0.0 all-gather.2.cloned.1.call-start
  29.8 0.0 copy-done.2
  29.8 0.0 copy-done.3
  29.8 0.7 pad_maximum_fusion
  30.6 0.0 all-gather.2.cloned.1.call-update
  30.6 0.0 copy-done.1
  30.6 0.4 multiply_reduce_fusion
  30.9 0.0 copy-done.4
  31.0 225.6 %all-gather.2.cloned.1.call-done = bf16[2048,1408]{1,0:T(8,128)(2,1)} async-done(((bf16[32,1408]{1,0:T(8,128)(2,1)}), bf16[2048,1408]{1,0:T(8,128)(2,1)}) %all-gather.2.cloned.1.call-update) | async-done | bytes 5767184 | tf_op jit(solution)/shard_map/all_gather | solution.py:60
  256.6 3.1 fusion.10
  259.7 0.0 all-to-all-done
  259.7 6.9 %fusion.12 = bf16[320,2048]{1,0:T(8,128)(2,1)} fusion(bf16[2048,960]{1,0:T(8,128)(2,1)} %bitcast.3, bf16[2048,1408]{1,0:T(8,128)(2,1)} %all-gather.2.cloned.1.call-done, f32[320,704]{1,0:T(8,128)S(1)} %fusion.10, f32[2048]{0:T(1024)S(1)} %bitcast.62, f32[320]{0:T(512)S(1)} %add_rsqrt_fusion, bf16[320,2048]{1,0:T(8,128)(2,1)S(1)} %copy-done.1), kind=kOutput, calls=%fused_computation.13 | convolution fusion | flops 1850122240 | bytes 9823488 | tf_op jit(solution)/shard_map/dot_general | solution.py:70
  266.6 8.2 %all-to-all-start.1 = ((bf16[8,40,2048]{2,1,0:T(8,128)(2,1)}), bf16[8,40,2048]{2,1,0:T(8,128)(2,1)S(1)}, u32[]{:S(2)}, u32[]{:S(2)}) async-start(bf16[8,40,2048]{2,1,0:T(8,128)(2,1)} %bitcast.49), calls=%async_computation.1 | async-start | bytes 2621440 | tf_op jit(solution)/shard_map/all_to_all | solution.py:24
  274.8 1.8 convert_element_type.82
  276.6 16.0 %all-to-all-done.1 = bf16[8,40,2048]{2,1,0:T(8,128)(2,1)S(1)} async-done(((bf16[8,40,2048]{2,1,0:T(8,128)(2,1)}), bf16[8,40,2048]{2,1,0:T(8,128)(2,1)S(1)}, u32[]{:S(2)}, u32[]{:S(2)}) %all-to-all-start.1) | async-done | bytes 1310752 | tf_op jit(solution)/shard_map/all_to_all | solution.py:24
  292.6 0.2 convert_reduce_fusion.2
  292.8 0.1 multiply_reduce_fusion.5
  292.9 0.0 copy-start.5
  292.9 1.2 multiply_reduce_fusion.4
  294.2 0.1 multiply_convert_fusion.5
  294.3 1.2 broadcast_in_dim.60
  295.5 4.4 %all-to-all-start.2 = ((bf16[8,40,2048]{2,1,0:T(8,128)(2,1)}), bf16[8,40,2048]{2,1,0:T(8,128)(2,1)S(1)}, u32[]{:S(2)}, u32[]{:S(2)}) async-start(bf16[8,40,2048]{2,1,0:T(8,128)(2,1)} %broadcast_in_dim.60), calls=%async_computation.2 | async-start | bytes 2621440 | tf_op jit(solution)/shard_map/all_to_all | solution.py:30
  299.9 0.0 copy-done.5
  300.0 17.8 %all-to-all-done.2 = bf16[8,40,2048]{2,1,0:T(8,128)(2,1)S(1)} async-done(((bf16[8,40,2048]{2,1,0:T(8,128)(2,1)}), bf16[8,40,2048]{2,1,0:T(8,128)(2,1)S(1)}, u32[]{:S(2)}, u32[]{:S(2)}) %all-to-all-start.2) | async-done | bytes 1310752 | tf_op jit(solution)/shard_map/all_to_all | solution.py:30
  317.7 1.8 convolution_convert_fusion.1
  319.6 0.1 fusion.50
  319.7 1.7 subtract_convert_fusion
  321.4 0.0 copy-done
  321.4 0.1 fusion.43
  321.6 0.0 slice-start
  321.6 2.0 convolution_convert_fusion
  323.5 21.1 %all_to_all.30 = bf16[8,40,2048]{2,1,0:T(8,128)(2,1)S(1)} all-to-all(bf16[8,40,2048]{2,1,0:T(8,128)(2,1)S(1)} %bitcast.45), channel_id=1, replica_groups=mesh['fs'=64,'tp'=8] {'tp'}, dimensions={0} | all-to-all | bytes 2621440 | tf_op jit(solution)/shard_map/all_to_all | solution.py:24
  344.7 0.0 slice-start.1
  344.7 0.2 convert_reduce_fusion.1
  344.9 0.1 multiply_reduce_fusion.3
  345.0 0.2 multiply_reduce_fusion.2
  345.3 0.1 multiply_convert_fusion.4
  345.4 0.1 broadcast_in_dim.68
  345.5 21.2 %all_to_all.31 = bf16[8,40,2048]{2,1,0:T(8,128)(2,1)S(1)} all-to-all(bf16[8,40,2048]{2,1,0:T(8,128)(2,1)S(1)} %broadcast_in_dim.68), channel_id=1, replica_groups=mesh['fs'=64,'tp'=8] {'tp'}, dimensions={0} | all-to-all | bytes 2621440 | tf_op jit(solution)/shard_map/all_to_all | solution.py:30
  366.8 0.0 slice-done
  366.8 0.0 slice-done.1
  366.8 2.2 fusion.8
  368.9 5.9 %fusion.15 = bf16[320,2048]{1,0:T(8,128)(2,1)S(1)} fusion(bf16[2048,960]{1,0:T(8,128)(2,1)} %bitcast.3, bf16[320,2048]{1,0:T(8,128)(2,1)S(1)} %bitcast.51, bf16[2048,1408]{1,0:T(8,128)(2,1)} %all-gather.2.cloned.1.call-done, f32[320,704]{1,0:T(8,128)} %fusion.8), kind=kOutput, calls=%fused_computation.14 | convolution fusion | flops 1847500800 | bytes 9895936 | tf_op jit(solution)/shard_map/dot_general | solution.py:70
  374.8 21.2 %all_to_all.32 = bf16[8,40,2048]{2,1,0:T(8,128)(2,1)S(1)} all-to-all(bf16[8,40,2048]{2,1,0:T(8,128)(2,1)S(1)} %bitcast.52), channel_id=1, replica_groups=mesh['fs'=64,'tp'=8] {'tp'}, dimensions={0} | all-to-all | bytes 2621440 | tf_op jit(solution)/shard_map/all_to_all | solution.py:24
  396.1 0.2 convert_reduce_fusion
  396.3 0.1 multiply_reduce_fusion.1
  396.4 0.8 add_convert_fusion
  (13 shorter events, 0.1 us)
Async XLA Ops:
  6.5 314.8 %copy-start = (bf16[1,128,128]{2,1,0:T(8,128)(2,1)S(1)}, bf16[1,128,128]{2,1,0:T(8,128)(2,1)}, u32[]{:S(2)}) copy-start(bf16[1,128,128]{2,1,0:T(8,128)(2,1)} %param.15) | copy-start | bytes 98308
  10.1 19.7 %copy-start.2 = (bf16[32,704]{1,0:T(8,128)(2,1)S(1)}, bf16[32,704]{1,0:T(8,128)(2,1)}, u32[]{:S(2)}) copy-start(bf16[32,704]{1,0:T(8,128)(2,1)} %param.11) | copy-start | bytes 135172
  10.1 19.8 %copy-start.3 = (bf16[32,704]{1,0:T(8,128)(2,1)S(1)}, bf16[32,704]{1,0:T(8,128)(2,1)}, u32[]{:S(2)}) copy-start(bf16[32,704]{1,0:T(8,128)(2,1)} %param.10) | copy-start | bytes 135172
  10.1 20.5 %copy-start.1 = (bf16[320,2048]{1,0:T(8,128)(2,1)S(1)}, bf16[320,2048]{1,0:T(8,128)(2,1)}, u32[]{:S(2)}) copy-start(bf16[320,2048]{1,0:T(8,128)(2,1)} %param.9) | copy-start | bytes 3932164
  10.1 20.9 %copy-start.4 = (f32[6,2048]{1,0:T(8,128)S(1)}, f32[6,2048]{1,0:T(8,128)}, u32[]{:S(2)}) copy-start(f32[6,2048]{1,0:T(8,128)} %param.17) | copy-start | bytes 147460
  10.1 249.6 %all-to-all-start = ((bf16[64,32,960]{2,1,0:T(8,128)(2,1)}), bf16[64,32,960]{2,1,0:T(8,128)(2,1)}, u32[]{:S(2)}, u32[]{:S(2)}) async-start(bf16[64,32,960]{2,1,0:T(8,128)(2,1)} %stack.2), calls=%async_computation | async-start | bytes 8388608 | tf_op jit(solution)/shard_map/all_to_all | solution.py:11
  29.8 226.8 %all-gather.2.cloned.1.call-start = ((), (), s32[]{:S(2)}) async-start(), calls=%async_computation.6 | async-start | bytes 5857280 | tf_op jit(solution)/shard_map/all_gather | solution.py:60
  266.6 26.0 %all-to-all-start.1 = ((bf16[8,40,2048]{2,1,0:T(8,128)(2,1)}), bf16[8,40,2048]{2,1,0:T(8,128)(2,1)S(1)}, u32[]{:S(2)}, u32[]{:S(2)}) async-start(bf16[8,40,2048]{2,1,0:T(8,128)(2,1)} %bitcast.49), calls=%async_computation.1 | async-start | bytes 2621440 | tf_op jit(solution)/shard_map/all_to_all | solution.py:24
  292.9 7.0 %copy-start.5 = (bf16[128]{0:T(256)(128)(2,1)S(1)}, bf16[128]{0:T(256)(128)(2,1)}, u32[]{:S(2)}) copy-start(bf16[128]{0:T(256)(128)(2,1)} %param.16) | copy-start | bytes 772
  295.5 22.2 %all-to-all-start.2 = ((bf16[8,40,2048]{2,1,0:T(8,128)(2,1)}), bf16[8,40,2048]{2,1,0:T(8,128)(2,1)S(1)}, u32[]{:S(2)}, u32[]{:S(2)}) async-start(bf16[8,40,2048]{2,1,0:T(8,128)(2,1)} %broadcast_in_dim.60), calls=%async_computation.2 | async-start | bytes 2621440 | tf_op jit(solution)/shard_map/all_to_all | solution.py:30
  321.6 45.2 %slice-start = ((s8[5767168]{0:T(1024)(128)(4,1)}), s8[4194304]{0:T(1024)(128)(4,1)S(1)}, s32[]{:S(2)}) async-start(s8[5767168]{0:T(1024)(128)(4,1)} %bitcast.63), calls=%async_computation.7 | async-start | bytes 8388608
  344.7 22.1 %slice-start.1 = ((s8[5767168]{0:T(1024)(128)(4,1)}), s8[1572864]{0:T(1024)(128)(4,1)S(1)}, s32[]{:S(2)}) async-start(s8[5767168]{0:T(1024)(128)(4,1)} %bitcast.63), calls=%async_computation.8 | async-start | bytes 3145728
Sparse Core Ops, SparseCore 0:
  33.5 222.9 all-gather.1
